TPU v7x, 32 devices: a whole 2x2x4 slice. The times are simulated.
32 devices in a mesh: sp: 4 (over z), fs: 4 (over y, x), tp: 2 (over core).
Axes of the slice: x: 2, y: 2, z: 4, core: 2. Of those that a mesh axis runs over, the one named last changes fastest.
Arguments:
- tokens: bfloat16 [4, 1024, 2048], P('fs', ('sp', 'tp')), may hold values from -6 to 6
- norm_gain: float32 [2048], replicated, may hold values from 0.1 to 1.9
- w_conv_gate: bfloat16 [2048, 1024], P('sp', 'tp'), may hold values from -0.125 to 0.125
- w_conv_in: bfloat16 [2048, 1024], P('sp', 'tp'), may hold values from -0.125 to 0.125
- w_conv_value: bfloat16 [2048, 1024], P('sp', 'tp'), may hold values from -0.125 to 0.125
- conv_taps: float32 [3, 1024], P(None, 'tp'), may hold values from -3.5 to 3.5
- w_receptance: bfloat16 [2048, 1024], P('sp', 'tp'), may hold values from -0.125 to 0.125
- w_key: bfloat16 [2048, 1024], P('sp', 'tp'), may hold values from -0.125 to 0.125
- w_value: bfloat16 [2048, 1024], P('sp', 'tp'), may hold values from -0.125 to 0.125
- w_decay_down: bfloat16 [2048, 128], P('sp'), may hold values from -0.125 to 0.125
- w_decay_up: bfloat16 [128, 1024], P(None, 'tp'), may hold values from -0.75 to 0.75
- decay_base: float32 [1024], P('tp'), may hold values from -12.5 to -3
- decay_shift: float32 [4, 1024, 1024], P('fs', 'sp', 'tp'), may hold values from -2.1 to 0
- w_rate_down: bfloat16 [2048, 128], P('sp'), may hold values from -0.125 to 0.125
- w_rate_up: bfloat16 [128, 1024], P(None, 'tp'), may hold values from -0.5 to 0.5
- rate_base: float32 [1024], P('tp'), may hold values from -10 to 1
- key_scale: float32 [1024], P('tp'), may hold values from 0.25 to 2.5
- key_mix: float32 [1024], P('tp'), may hold values from 0.1 to 0.7
- group_gain: float32 [1024], P('tp'), may hold values from 0.1 to 1.9
- w_out_conv: bfloat16 [1024, 2048], P('tp', 'sp'), may hold values from -0.125 to 0.125
- w_out_state: bfloat16 [1024, 2048], P('tp', 'sp'), may hold values from -0.125 to 0.125
Outputs:
- mixed: bfloat16 [4, 1024, 2048], P('fs', ('sp', 'tp'))
All inputs are finite; a program needn't handle non-finite values.
Results may differ from a plain program's by a relative error of at most 0.015.
Values may be sent and summed in bfloat16 or wider, within the bound.
A program may use at most 128 MiB of HBM per device.

v0:
```python
import functools

import jax
import jax.numpy as jnp
from jax import lax
from jax.experimental import pallas as pl
from jax.experimental.pallas import tpu as pltpu
from jax.sharding import PartitionSpec as P

HEAD = 64
CHUNK = 64
norm_eps = 1e-06
group_eps = 0.00064
f32, bf16 = jnp.float32, jnp.bfloat16

NN = (((1,), (0,)), ((), ()))
NT = (((1,), (1,)), ((), ()))
TN = (((0,), (0,)), ((), ()))


def dot1(a, b, dims):
    return lax.dot_general(a.astype(bf16), b.astype(bf16), dims, preferred_element_type=f32)


def dot3(a, b, dims):
    ah, bh = a.astype(bf16), b.astype(bf16)
    al, bl = (a - ah.astype(f32)).astype(bf16), (b - bh.astype(f32)).astype(bf16)
    d = functools.partial(lax.dot_general, dimension_numbers=dims, preferred_element_type=f32)
    return d(ah, bh) + (d(ah, bl) + d(al, bh))


def stack_heads(x, lanes_low):
    return jnp.concatenate([jnp.where(lanes_low, x, 0.0), jnp.where(lanes_low, 0.0, x)], axis=0)


def fold(x):
    half = x.shape[0] // 2
    return x[:half] + x[half:]


def state_kernel(
    recv_ref, key_ref, val_ref, dlow_ref, rlow_ref, wdu_ref, wru_ref, shift_ref, par_ref,
    q_ref, l_ref, ma_ref,
):
    tokens, width = recv_ref.shape
    par = par_ref[...]
    decay_base, rate_base, key_scale, key_mix = (par[i : i + 1] for i in range(4))
    act = jnp.tanh(dlow_ref[...].astype(f32)).astype(bf16)
    pre = decay_base + lax.dot_general(act, wdu_ref[...], NN, preferred_element_type=f32)
    log_decay = shift_ref[0] - jnp.exp(-0.5) * jax.nn.sigmoid(pre)
    rate = jax.nn.sigmoid(
        rate_base + lax.dot_general(rlow_ref[...], wru_ref[...], NN, preferred_element_type=f32)
    )
    key = key_ref[...].astype(f32)
    scaled = key * key_scale
    lane_low = lax.broadcasted_iota(jnp.int32, (1, width), 1) < HEAD
    sq = scaled * scaled
    low_sum = jnp.sum(jnp.where(lane_low, sq, 0.0), axis=-1, keepdims=True)
    high_sum = jnp.sum(jnp.where(lane_low, 0.0, sq), axis=-1, keepdims=True)
    erase = scaled * lax.rsqrt(jnp.where(lane_low, low_sum, high_sum) + norm_eps)
    write = key * (1.0 + (rate - 1.0) * key_mix)
    replace = erase * rate
    recv = recv_ref[...].astype(f32)
    val = val_ref[...].astype(f32)

    rows = 2 * CHUNK
    ri = lax.broadcasted_iota(jnp.int32, (rows, rows), 0)
    ci = lax.broadcasted_iota(jnp.int32, (rows, rows), 1)
    same = (ri < CHUNK) == (ci < CHUNK)
    strict = jnp.logical_and(same, ri > ci)
    causal = jnp.logical_and(same, ri >= ci)
    eye = (ri == ci).astype(f32)
    tri = jnp.where(
        lax.broadcasted_iota(jnp.int32, (CHUNK, CHUNK), 0)
        >= lax.broadcasted_iota(jnp.int32, (CHUNK, CHUNK), 1),
        1.0,
        0.0,
    ).astype(f32)
    wi = lax.broadcasted_iota(jnp.int32, (width, width), 0)
    wj = lax.broadcasted_iota(jnp.int32, (width, width), 1)
    weye = wi == wj

    parts = []
    for c in range(tokens // CHUNK):
        sl = slice(c * CHUNK, (c + 1) * CHUNK)
        ld = log_decay[sl]
        incl = lax.dot_general(tri, ld, NN, precision=lax.Precision.HIGHEST, preferred_element_type=f32)
        final = incl[CHUNK - 1 : CHUNK]
        mid = incl[CHUNK // 2 - 1 : CHUNK // 2]
        excl = incl - ld
        up, back = jnp.exp(incl - mid), jnp.exp(mid - incl)
        st = lambda x: stack_heads(x, lane_low)
        e_mid = st(-erase[sl] * jnp.exp(excl - mid))
        q_mid = st(recv[sl] * up)
        r_back = st(replace[sl] * back)
        k_back = st(write[sl] * back)
        v = st(val[sl])
        e_now = st(-erase[sl] * jnp.exp(excl))
        q_now = st(recv[sl] * jnp.exp(incl))
        tail = jnp.exp(final - incl)
        r_end = st(replace[sl] * tail)
        k_end = st(write[sl] * tail)
        x = jnp.where(strict, dot3(e_mid, r_back, NT), 0.0)
        ek = jnp.where(strict, dot1(e_mid, k_back, NT), 0.0)
        qr = jnp.where(causal, dot1(q_mid, r_back, NT), 0.0)
        qk = jnp.where(causal, dot1(q_mid, k_back, NT), 0.0)
        inv = eye + x
        power = x
        reached = 2
        while reached < CHUNK:
            power = dot3(power, power, NN)
            inv = inv + dot3(inv, power, NN)
            reached *= 2
        start_map = dot3(inv, e_now, NN)
        local_erase = dot1(inv, dot1(ek, v, NN), NN)
        query_map = fold(q_now + dot1(qr, start_map, NN))
        local_out = fold(dot1(qr, local_erase, NN) + dot1(qk, v, NN))
        decay_diag = jnp.where(weye, jnp.exp(final), 0.0)
        step_map = decay_diag + dot3(start_map, r_end, TN)
        carried = dot1(local_erase, r_end, TN) + dot1(v, k_end, TN)
        parts.append((query_map, local_out, step_map, carried))

    total_map = total_add = None
    for c, (query_map, local_out, step_map, carried) in enumerate(parts):
        sl = slice(c * CHUNK, (c + 1) * CHUNK)
        if c == 0:
            q_ref[sl] = query_map.astype(bf16)
            l_ref[sl] = local_out
            total_map, total_add = step_map, carried
        else:
            q_ref[sl] = dot1(query_map, total_map, NT).astype(bf16)
            l_ref[sl] = local_out + dot1(query_map, total_add, NT)
            total_map, total_add = (
                dot3(total_map, step_map, NN),
                dot3(total_add, step_map, NN) + carried,
            )
    ma_ref[0, 0] = fold(total_map).astype(bf16)
    ma_ref[0, 1] = fold(total_add).astype(bf16)


def finish_kernel(n_sp, place_ref, q_ref, l_ref, ma_ref, gain_ref, out_ref):
    width = q_ref.shape[1]
    place = place_ref[0]
    wi = lax.broadcasted_iota(jnp.int32, (width, width), 0)
    wj = lax.broadcasted_iota(jnp.int32, (width, width), 1)
    same = (wi < HEAD) == (wj < HEAD)
    widen = lambda x: jnp.where(same, jnp.concatenate([x, x], axis=0), 0.0)
    state = jnp.zeros((width, width), f32)
    for hop in range(n_sp - 1):
        new = dot3(state, widen(ma_ref[hop, 0, 0].astype(f32)), NN) + widen(
            ma_ref[hop, 0, 1].astype(f32)
        )
        state = jnp.where(hop < place, new, state)
    out = l_ref[...] + dot1(q_ref[...], state, NT)
    low = lax.broadcasted_iota(jnp.int32, (1, width), 1) < HEAD

    def head_mean(x):
        a = jnp.sum(jnp.where(low, x, 0.0), axis=-1, keepdims=True)
        b = jnp.sum(jnp.where(low, 0.0, x), axis=-1, keepdims=True)
        return jnp.where(low, a, b) * (1.0 / HEAD)

    centered = out - head_mean(out)
    var = head_mean(centered * centered)
    out_ref[...] = (centered * lax.rsqrt(var + group_eps) * gain_ref[...]).astype(bf16)


def normalize_rows(norm_gain, row_piece):
    values = row_piece.astype(f32)
    scaled = values * lax.rsqrt(jnp.mean(values * values, axis=-1, keepdims=True) + norm_eps)
    return (scaled * norm_gain).astype(bf16)


def body(
    tokens, norm_gain, w_conv_gate, w_conv_in, w_conv_value, conv_taps, w_receptance, w_key,
    w_value, w_decay_down, w_decay_up, decay_base, decay_shift, w_rate_down, w_rate_up,
    rate_base, key_scale, key_mix, group_gain, w_out_conv, w_out_state,
):
    n_fs, n_sp = lax.axis_size("fs"), lax.axis_size("sp")
    fs = lax.axis_index("fs")
    width = w_key.shape[1] // n_fs

    def mine(a, axis):
        return lax.dynamic_slice_in_dim(a, fs * width, width, axis)

    normed = lax.all_gather(normalize_rows(norm_gain, tokens[0]), ("fs", "tp"), axis=0, tiled=True)
    steps = normed.shape[0] // n_fs
    w_state = jnp.concatenate(
        [mine(w_receptance, 1), mine(w_key, 1), mine(w_value, 1), w_decay_down, w_rate_down], axis=1
    )
    w_conv = jnp.concatenate([mine(w_conv_gate, 1), mine(w_conv_in, 1), mine(w_conv_value, 1)], axis=1)
    w_out = jnp.concatenate([mine(w_out_conv, 0), mine(w_out_state, 0)], axis=0)
    w_state = lax.all_gather(w_state, "sp", axis=0, tiled=True)
    w_conv = lax.all_gather(w_conv, "sp", axis=0, tiled=True)
    w_out = lax.all_gather(w_out, "sp", axis=0)
    shift = lax.all_to_all(
        decay_shift[0].reshape(steps, n_fs, width), "fs", split_axis=1, concat_axis=0
    ).reshape(n_fs, steps, width)

    state_in = jnp.dot(normed, w_state, preferred_element_type=f32).astype(bf16)
    params = jnp.stack([mine(p, 0) for p in (decay_base, rate_base, key_scale, key_mix)])
    rank = w_decay_down.shape[1]
    col = lambda k: pl.BlockSpec((steps, width), lambda i, k=k: (i, k))
    low = lambda k: pl.BlockSpec((steps, rank), lambda i, k=k: (i, 3 * width // rank + k))
    full = lambda s: pl.BlockSpec(s, lambda i: (0,) * len(s))
    query, local, ma = pl.pallas_call(
        state_kernel,
        grid=(n_fs,),
        in_specs=[
            col(0), col(1), col(2), low(0), low(1), full((rank, width)), full((rank, width)),
            pl.BlockSpec((1, steps, width), lambda i: (i, 0, 0)), full((4, width)),
        ],
        out_specs=[
            col(0), col(0), pl.BlockSpec((1, 2, HEAD, width), lambda i: (i, 0, 0, 0)),
        ],
        out_shape=[
            jax.ShapeDtypeStruct((n_fs * steps, width), bf16),
            jax.ShapeDtypeStruct((n_fs * steps, width), f32),
            jax.ShapeDtypeStruct((n_fs, 2, HEAD, width), bf16),
        ],
        cost_estimate=pl.CostEstimate(flops=40_000_000_000, bytes_accessed=4_000_000, transcendentals=0),
    )(
        state_in, state_in, state_in, state_in, state_in, mine(w_decay_up, 1), mine(w_rate_up, 1),
        shift, params,
    )
    ma_all = lax.all_gather(ma, "sp", axis=0)

    conv = jnp.dot(normed, w_conv, preferred_element_type=f32).astype(bf16)
    gate, source, value = (
        conv[:, i * width : (i + 1) * width].reshape(n_fs, steps, width) for i in range(3)
    )
    route = [(i, i + 1) for i in range(n_sp - 1)]
    previous = lax.ppermute(jnp.stack([source[:, -2:], value[:, -2:]]), "sp", route)
    product = jnp.concatenate([previous[0], source], axis=1).astype(f32) * jnp.concatenate(
        [previous[1], value], axis=1
    ).astype(f32)
    taps = mine(conv_taps, 1)
    filtered = taps[0] * product[:, :-2] + taps[1] * product[:, 1:-1] + taps[2] * product[:, 2:]
    conv_out = (gate.astype(f32) * filtered).astype(bf16).reshape(n_fs * steps, width)

    state_out = pl.pallas_call(
        functools.partial(finish_kernel, n_sp),
        grid=(n_fs,),
        in_specs=[
            pl.BlockSpec(memory_space=pltpu.SMEM), col(0), col(0),
            pl.BlockSpec((n_sp, 1, 2, HEAD, width), lambda i: (0, i, 0, 0, 0)), full((1, width)),
        ],
        out_specs=col(0),
        out_shape=jax.ShapeDtypeStruct((n_fs * steps, width), bf16),
    )(lax.axis_index("sp").reshape(1), query, local, ma_all, mine(group_gain, 0)[None])

    both = jnp.concatenate([conv_out, state_out], axis=1)
    partial = jnp.concatenate(
        [jnp.dot(both, w_out[j], preferred_element_type=f32).astype(bf16) for j in range(n_sp)], axis=1
    )
    mixed = lax.psum_scatter(partial, ("fs", "tp"), scatter_dimension=0, tiled=True)
    return mixed[None]


def solution(mesh):
    in_specs = (
        P("fs", ("sp", "tp"), None), P(), P("sp", "tp"), P("sp", "tp"), P("sp", "tp"),
        P(None, "tp"), P("sp", "tp"), P("sp", "tp"), P("sp", "tp"), P("sp", None), P(None, "tp"),
        P("tp"), P("fs", "sp", "tp"), P("sp", None), P(None, "tp"), P("tp"), P("tp"), P("tp"),
        P("tp"), P("tp", "sp"), P("tp", "sp"),
    )
    out_specs = P("fs", ("sp", "tp"), None)
    return jax.shard_map(body, mesh=mesh, in_specs=in_specs, out_specs=out_specs, check_vma=False)
```

profile of v0, /device:TPU:25, one launch (start us, length us, event | category | flops | bytes accessed | tf_op | source)
XLA Modules:
  0.0 279.7 jit_solution(6468520719808332910)
XLA Ops:
  6.5 0.0 all-gather.9.cloned.1.call-start
  6.6 1.0 copy-done
  7.6 1.0 constant_dynamic-slice_fusion.5
  8.6 0.8 pad_maximum_fusion.2
  9.4 0.0 all-gather.7.cloned.1.call-start
  9.5 1.2 fusion
  10.7 2.0 fusion.2
  12.8 0.0 all-gather.11.cloned.1.call-start
  12.8 0.9 dynamic-slice_dynamic-update-slice_fusion.2
  13.8 0.9 dynamic-slice_dynamic-update-slice_fusion.1
  14.7 0.9 dynamic-slice_dynamic-update-slice_fusion
  15.8 0.8 copy-done.2
  16.6 0.2 copy.26
  16.8 1.0 copy.27
  17.8 3.5 %all-to-all-start = ((f32[1,256,4,128]{3,1,0,2:T(8,128)}), f32[1,256,4,128]{3,1,0,2:T(8,128)S(1)}, u32[]{:S(2)}, u32[]{:S(2)}) async-start(f32[1,256,4,128]{3,1,0,2:T(8,128)} %copy.27), calls=%async_computation | async-start | bytes 1048576 | tf_op jit(solution)/shard_map/all_to_all | solution.py:195
  21.3 0.0 all-gather.13.cloned.1.call-start
  21.4 1.0 constant_dynamic-slice_fusion
  22.4 0.7 pad_maximum_fusion.3
  23.1 0.0 reduce-scatter.4.cloned.1.call-start
  23.1 0.7 constant_dynamic-slice_fusion.4
  23.8 1.3 dynamic-slice_bitcast_fusion.gain_ref
  25.1 0.8 dynamic-slice_bitcast_fusion.1
  25.9 0.8 dynamic-slice_bitcast_fusion.3
  26.7 1.4 constant_dynamic-slice_fusion.2
  28.1 0.6 pad_maximum_fusion.5.par_ref
  28.7 16.8 %all-gather.9.cloned.1.call-done = bf16[2048,384]{1,0:T(8,128)(2,1)} async-done(((bf16[512,384]{1,0:T(8,128)(2,1)}), bf16[2048,384]{1,0:T(8,128)(2,1)}) %all-gather.9.cloned.1.call-update) | async-done | bytes 1572880 | tf_op jit(solution)/shard_map/all_gather | solution.py:193
  45.4 39.9 %all-gather.7.cloned.1.call-done = bf16[1024,2048]{1,0:T(8,128)(2,1)} async-done(((bf16[128,2048]{1,0:T(8,128)(2,1)}), bf16[1024,2048]{1,0:T(8,128)(2,1)}) %all-gather.7.cloned.1.call-update) | async-done | bytes 4194320 | tf_op jit(solution)/shard_map/all_gather | solution.py:185
  85.4 5.0 %convolution_convert_fusion.5 = bf16[1024,384]{1,0:T(8,128)(2,1)S(1)} fusion(bf16[1024,2048]{1,0:T(8,128)(2,1)} %all-gather.7.cloned.1.call-done, bf16[2048,384]{1,0:T(8,128)(2,1)} %all-gather.9.cloned.1.call-done), kind=kOutput, calls=%fused_computation.6 | convolution fusion | flops 1611005952 | bytes 6553600 | tf_op jit(solution)/shard_map/dot_general | solution.py:227
  90.4 0.1 fusion.11
  90.6 1.3 collective-permute-start
  91.9 47.1 %all-gather.11.cloned.1.call-done = bf16[2048,640]{1,0:T(8,128)(2,1)} async-done(((bf16[512,640]{1,0:T(8,128)(2,1)}), bf16[2048,640]{1,0:T(8,128)(2,1)}) %all-gather.11.cloned.1.call-update) | async-done | bytes 2621456 | tf_op jit(solution)/shard_map/all_gather | solution.py:192
  139.0 7.5 %convolution_convert_fusion.recv_ref.key_ref.val_ref.dlow_ref.rlow_ref = bf16[1024,640]{1,0:T(8,128)(2,1)} fusion(bf16[1024,2048]{1,0:T(8,128)(2,1)} %all-gather.7.cloned.1.call-done, bf16[2048,640]{1,0:T(8,128)(2,1)} %all-gather.11.cloned.1.call-done), kind=kOutput, calls=%fused_computation.1 | convolution fusion | flops 2685009920 | bytes 8126464 | tf_op jit(solution)/shard_map/dot_general | solution.py:199
  146.6 0.8 copy-done.4
  147.3 33.8 %shard_map.199 = (bf16[1024,128]{1,0:T(8,128)(2,1)}, f32[1024,128]{1,0:T(8,128)}, bf16[4,2,64,128]{3,2,1,0:T(8,128)(2,1)}) custom-call(bf16[1024,640]{1,0:T(8,128)(2,1)} %convolution_convert_fusion.recv_ref.key_ref.val_ref.dlow_ref.rlow_ref, bf16[1024,640]{1,0:T(8,128)(2,1)} %convolution_convert_fusion.recv_ref.key_ref.val_ref.dlow_ref.rlow_ref, ...), custom_call_target="tpu_custom_call" | custom-call | flops 40000000000 | bytes 4000000 | tf_op jit(solution)/shard_map/pallas_call | solution.py:205
  181.2 14.4 %all-gather = bf16[16,2,64,128]{3,2,1,0:T(8,128)(2,1)} all-gather(bf16[4,2,64,128]{3,2,1,0:T(8,128)(2,1)} %get-tuple-element.10), channel_id=2, replica_groups=mesh['sp'=4,'fs'=4,'tp'=2] {'sp'}, dimensions={0}, use_global_device_ids=true | all-gather | bytes 655360 | tf_op jit(solution)/shard_map/all_gather | solution.py:225
  195.6 5.4 %shard_map.200 = bf16[1024,128]{1,0:T(8,128)(2,1)} custom-call(s32[1]{0:T(128)} %bitcast.13.place_ref, bf16[1024,128]{1,0:T(8,128)(2,1)} %get-tuple-element.8.q_ref, f32[1024,128]{1,0:T(8,128)} %get-tuple-element.9.l_ref, bf16[4,4,2,64,128]{4,3,2,1,0:T(8,128)(2,1)} %bitcast.51, f32[1,128]{1,0:T(1,128)} %dynamic-slice_bitcast_fusion.gain_ref), custom_call_target="tpu_custom_call" | custom-call | tf_op jit(solution)/shard_map/pallas_call | solution.py:240
  201.0 0.1 convert_multiply_fusion.2
  201.1 0.2 fusion.5
  201.3 0.0 all-gather.13.cloned.1.call-done
  201.3 1.5 convolution_convert_fusion.4
  202.9 1.4 convolution_convert_fusion.3
  204.3 1.4 convolution_convert_fusion.2
  205.8 1.4 convolution_convert_fusion.1
  207.2 2.4 pad_maximum_fusion
  209.6 6.5 %copy.29 = bf16[1024,2048]{1,0:T(8,128)(2,1)} copy(bf16[1024,2048]{0,1:T(8,128)(2,1)} %pad_maximum_fusion) | data formatting | bytes 8388608
  216.1 54.7 %reduce-scatter.4.cloned.1.call-done = bf16[128,2048]{1,0:T(8,128)(2,1)} async-done(((bf16[1024,2048]{1,0:T(8,128)(2,1)}), bf16[128,2048]{1,0:T(8,128)(2,1)}) %reduce-scatter.4.cloned.1.call-update) | async-done | bytes 524304
  270.8 1.3 copy.30
  272.2 1.0 copy.28
  (27 shorter events, 0.2 us)
Async XLA Ops:
  6.5 1.0 copy-start
  6.5 9.1 %copy-start.5 = (bf16[512,128]{1,0:T(8,128)(2,1)S(1)}, bf16[512,128]{1,0:T(8,128)(2,1)}, u32[]{:S(2)}) copy-start(bf16[512,128]{1,0:T(8,128)(2,1)} %param.30) | copy-start | bytes 393220
  6.5 9.2 %copy-start.6 = (bf16[512,128]{1,0:T(8,128)(2,1)S(1)}, bf16[512,128]{1,0:T(8,128)(2,1)}, u32[]{:S(2)}) copy-start(bf16[512,128]{1,0:T(8,128)(2,1)} %param.34) | copy-start | bytes 393220
  6.5 10.1 %copy-start.3 = (f32[1,256,512]{2,1,0:T(8,128)S(1)}, f32[1,256,512]{2,1,0:T(8,128)}, u32[]{:S(2)}) copy-start(f32[1,256,512]{2,1,0:T(8,128)} %param.33) | copy-start | bytes 1572868
  6.5 38.9 %all-gather.9.cloned.1.call-start = ((), (), s32[]{:S(2)}) async-start(), calls=%async_computation.3 | async-start | bytes 1966080 | tf_op jit(solution)/shard_map/all_gather | solution.py:193
  9.4 75.9 %all-gather.7.cloned.1.call-start = ((), (), s32[]{:S(2)}) async-start(), calls=%async_computation.2 | async-start | bytes 4718592 | tf_op jit(solution)/shard_map/all_gather | solution.py:185
  12.8 126.2 %all-gather.11.cloned.1.call-start = ((), (), s32[]{:S(2)}) async-start(), calls=%async_computation.4 | async-start | bytes 3276800 | tf_op jit(solution)/shard_map/all_gather | solution.py:192
  15.8 0.8 copy-start.2
  17.8 128.7 %all-to-all-start = ((f32[1,256,4,128]{3,1,0,2:T(8,128)}), f32[1,256,4,128]{3,1,0,2:T(8,128)S(1)}, u32[]{:S(2)}, u32[]{:S(2)}) async-start(f32[1,256,4,128]{3,1,0,2:T(8,128)} %copy.27), calls=%async_computation | async-start | bytes 1048576 | tf_op jit(solution)/shard_map/all_to_all | solution.py:195
  21.3 180.0 %all-gather.13.cloned.1.call-start = ((), (), s32[]{:S(2)}) async-start(), calls=%async_computation.5 | async-start | bytes 1310720 | tf_op jit(solution)/shard_map/all_gather | solution.py:194
  23.1 247.7 %reduce-scatter.4.cloned.1.call-start = ((), (), s32[]{:S(2)}) async-start(), calls=%async_computation.6 | async-start | bytes 4718592
  90.6 110.4 %collective-permute-start = (bf16[2,4,2,128]{3,2,1,0:T(2,128)(2,1)S(1)}, bf16[2,4,2,128]{3,2,1,0:T(2,128)(2,1)S(1)}, u32[]{:S(2)}, u32[]{:S(2)}) collective-permute-start(bf16[2,4,2,128]{3,2,1,0:T(2,128)(2,1)S(1)} %pad_maximum_fusion.4), channel_id=1, source_target_pairs={{0,8},{8,16},{16,24},{1,9},{9,17},{17,25},{2,10},{10,18},{18,26},{... | collective-permute-start | bytes 12296 | tf_op jit(solution)/shard_map/ppermute | solution.py:232
  146.6 0.8 copy-start.4
  200.9 1.9 copy-start.1
Sparse Core Ops, SparseCore 0:
  9.6 35.8 all-gather.8
  47.3 38.0 all-gather.6
  86.9 52.0 all-gather.10
  140.4 27.3 all-gather.12
  216.2 54.5 reduce-scatter.3
where the time goes:
time: 283 us; the launch traced here: 280 us
  waiting for transfers between devices  159 us (56%)
  Pallas kernels  39.2 us (14%)
  local copies, waits for them, and re-layouts  22.6 us (8%)
  matrix products  18.3 us (6%)
  blocking collectives  14.4 us (5%)
  between operations  13.4 us (5%)
  other arithmetic  8.12 us (3%)
  starting transfers between devices  4.96 us (2%)
    unnamed x6, waiting for transfers between devices  54.8 us
    all_gather x1, waiting for transfers between devices, body(): w_state = lax.all_gather(w_state, 'sp', axis=0, tiled=True)  47.1 us
    all_gather x1, waiting for transfers between devices, body(): lax.all_gather(normalize_rows(norm_gain, tokens[0]), ('fs', 'tp'), axis=0...  39.9 us
    pallas_call x1, Pallas kernels, body(): pl.pallas_call(state_kernel, grid=(n_fs,), in_specs=[col(0), col(1), col(...  33.8 us
    all_gather x1, waiting for transfers between devices, body(): w_conv = lax.all_gather(w_conv, 'sp', axis=0, tiled=True)  16.8 us
    all_gather x1, blocking collectives, body(): ma_all = lax.all_gather(ma, 'sp', axis=0)  14.4 us
    unnamed x21, local copies, waits for them, and re-layouts  13.5 us
    dot_general x1, matrix products, body(): state_in = jnp.dot(normed, w_state, preferred_element_type=f32).astype(bf16)  7.53 us
  transfers between devices with their start and end apart: 7, of which 4 were waited for; matrix products, arithmetic and copies ran while one was open for 10% of the time, Pallas kernels for 14%

commit v1 on v0

--- a/solution.py
+++ b/solution.py
@@ -164,6 +164,199 @@
     out_ref[...] = (centered * lax.rsqrt(var + group_eps) * gain_ref[...]).astype(bf16)
 
 
+MESH = pl.DeviceIdType.MESH
+
+
+def greet(peers):
+    barrier = pltpu.get_barrier_semaphore()
+    for peer in peers:
+        pl.semaphore_signal(barrier, inc=1, device_id=peer, device_id_type=MESH)
+    return barrier
+
+
+def send(src, dst, send_sem, recv_sem, peer):
+    return pltpu.make_async_remote_copy(
+        src_ref=src, dst_ref=dst, send_sem=send_sem, recv_sem=recv_sem,
+        device_id=peer, device_id_type=MESH,
+    )
+
+
+def gather_kernel(
+    n_sp, n_fs, tok_ref, w_ref, toks, weights, local_sem, tok_send, tok_recv, pair_send, pair_recv,
+    right_send, left_send, w_recv,
+):
+    sp, fs, tp = lax.axis_index("sp"), lax.axis_index("fs"), lax.axis_index("tp")
+    partner = {"tp": 1 - tp}
+    others = [lax.rem(fs + d, n_fs) for d in range(1, n_fs)]
+    barrier = greet([partner] + [{"fs": f} for f in others])
+    has_left, has_right = sp > 0, sp < n_sp - 1
+
+    @pl.when(has_left)
+    def _():
+        pl.semaphore_signal(barrier, inc=1, device_id={"sp": sp - 1}, device_id_type=MESH)
+
+    @pl.when(has_right)
+    def _():
+        pl.semaphore_signal(barrier, inc=1, device_id={"sp": sp + 1}, device_id_type=MESH)
+
+    pl.semaphore_wait(barrier, n_fs + has_left.astype(jnp.int32) + has_right.astype(jnp.int32))
+
+    def rightward(j):
+        src = weights.at[j]
+        return send(src, weights.at[j], right_send.at[j], w_recv.at[j], {"sp": sp + 1})
+
+    def leftward(j):
+        src = weights.at[j]
+        return send(src, weights.at[j], left_send.at[j], w_recv.at[j], {"sp": sp - 1})
+
+    own_right = send(w_ref, weights.at[sp], right_send.at[sp], w_recv.at[sp], {"sp": sp + 1})
+    own_left = send(w_ref, weights.at[sp], left_send.at[sp], w_recv.at[sp], {"sp": sp - 1})
+
+    @pl.when(has_right)
+    def _():
+        own_right.start()
+
+    @pl.when(has_left)
+    def _():
+        own_left.start()
+
+    own_w = pltpu.make_async_copy(w_ref, weights.at[sp], local_sem.at[0])
+    own_t = pltpu.make_async_copy(tok_ref, toks.at[fs, tp], local_sem.at[1])
+    own_w.start()
+    own_t.start()
+    token_sends = [
+        send(tok_ref, toks.at[fs, tp], tok_send.at[f], tok_recv.at[fs], {"fs": f}) for f in others
+    ]
+    for copy in token_sends:
+        copy.start()
+    pair_own = send(tok_ref, toks.at[fs, tp], pair_send.at[fs], pair_recv.at[fs], partner)
+    pair_own.start()
+
+    def from_peer(f):
+        return send(toks.at[f, tp], toks.at[f, tp], tok_send.at[f], tok_recv.at[f], {"fs": f})
+
+    def to_partner(f):
+        return send(toks.at[f, tp], toks.at[f, tp], pair_send.at[f], pair_recv.at[f], partner)
+
+    def from_partner(f):
+        there = toks.at[f, 1 - tp]
+        return send(there, there, pair_send.at[f], pair_recv.at[f], partner)
+
+    for k in range(1, n_sp):
+
+        @pl.when(sp >= k)
+        def _():
+            rightward(sp - k).wait_recv()
+
+            @pl.when(has_right)
+            def _():
+                rightward(sp - k).start()
+
+        @pl.when(sp + k < n_sp)
+        def _():
+            leftward(sp + k).wait_recv()
+
+            @pl.when(has_left)
+            def _():
+                leftward(sp + k).start()
+
+        if k == 1:
+            for f in reversed(others):
+                from_peer(f).wait_recv()
+                to_partner(f).start()
+
+    own_w.wait()
+    own_t.wait()
+    for copy in token_sends:
+        copy.wait_send()
+    pair_own.wait_send()
+    for f in others:
+        to_partner(f).wait_send()
+    for f in [fs] + others:
+        from_partner(f).wait_recv()
+
+    @pl.when(has_right)
+    def _():
+        own_right.wait_send()
+
+    @pl.when(has_left)
+    def _():
+        own_left.wait_send()
+
+    for k in range(1, n_sp):
+
+        @pl.when(jnp.logical_and(sp >= k, has_right))
+        def _():
+            rightward(sp - k).wait_send()
+
+        @pl.when(jnp.logical_and(sp + k < n_sp, has_left))
+        def _():
+            leftward(sp + k).wait_send()
+
+
+def reduce_kernel(
+    n_fs, part_ref, out_ref, from_pair, sums, from_fs, pair_send, pair_recv, fs_send, fs_recv
+):
+    fs, tp = lax.axis_index("fs"), lax.axis_index("tp")
+    partner = {"tp": 1 - tp}
+    order = [lax.rem(fs + d, n_fs) for d in range(1, n_fs)] + [fs]
+    barrier = greet([partner] + [{"fs": f} for f in order[:-1]])
+    pl.semaphore_wait(barrier, n_fs)
+    swaps = [
+        send(part_ref.at[f, 1 - tp], from_pair.at[d], pair_send.at[d], pair_recv.at[d], partner)
+        for d, f in enumerate(order)
+    ]
+    for copy in swaps:
+        copy.start()
+    sends = []
+    for d, f in enumerate(order):
+        swaps[d].wait_recv()
+        total = part_ref[f, tp].astype(f32) + from_pair[d].astype(f32)
+        sums[d] = total.astype(bf16)
+        if d < n_fs - 1:
+            copy = send(sums.at[d], from_fs.at[d], fs_send.at[d], fs_recv.at[d], {"fs": f})
+            copy.start()
+            sends.append(copy)
+    for copy in sends:
+        copy.wait_recv()
+    result = sums[n_fs - 1].astype(f32)
+    for d in range(n_fs - 1):
+        result = result + from_fs[d].astype(f32)
+    out_ref[...] = result.astype(bf16)
+    for copy in sends:
+        copy.wait_send()
+    for copy in swaps:
+        copy.wait_send()
+
+
+def gather_inputs(n_sp, n_fs, n_tp, tok, w):
+    dma = lambda n: pltpu.SemaphoreType.DMA((n,))
+    return pl.pallas_call(
+        functools.partial(gather_kernel, n_sp, n_fs),
+        in_specs=[pl.BlockSpec(memory_space=pltpu.VMEM)] * 2,
+        out_specs=[pl.BlockSpec(memory_space=pltpu.VMEM)] * 2,
+        out_shape=[
+            jax.ShapeDtypeStruct((n_fs, n_tp) + tok.shape, bf16),
+            jax.ShapeDtypeStruct((n_sp,) + w.shape, bf16),
+        ],
+        scratch_shapes=[dma(2), dma(n_fs), dma(n_fs), dma(n_fs), dma(n_fs), dma(n_sp), dma(n_sp), dma(n_sp)],
+        compiler_params=pltpu.CompilerParams(collective_id=0, has_side_effects=True),
+    )(tok, w)
+
+
+def reduce_partials(n_fs, part):
+    dma = pltpu.SemaphoreType.DMA((n_fs,))
+    block = pltpu.VMEM((n_fs,) + part.shape[2:], bf16)
+    return pl.pallas_call(
+        functools.partial(reduce_kernel, n_fs),
+        in_specs=[pl.BlockSpec(memory_space=pltpu.VMEM)],
+        out_specs=pl.BlockSpec(memory_space=pltpu.VMEM),
+        out_shape=jax.ShapeDtypeStruct(part.shape[2:], bf16),
+        scratch_shapes=[block, block, block, dma, dma, dma, dma],
+        compiler_params=pltpu.CompilerParams(collective_id=1, has_side_effects=True),
+    )(part)
+
+
 def normalize_rows(norm_gain, row_piece):
     values = row_piece.astype(f32)
     scaled = values * lax.rsqrt(jnp.mean(values * values, axis=-1, keepdims=True) + norm_eps)
@@ -182,19 +375,23 @@
     def mine(a, axis):
         return lax.dynamic_slice_in_dim(a, fs * width, width, axis)
 
-    normed = lax.all_gather(normalize_rows(norm_gain, tokens[0]), ("fs", "tp"), axis=0, tiled=True)
-    steps = normed.shape[0] // n_fs
+    n_tp = lax.axis_size("tp")
+    steps = decay_shift.shape[1]
     w_state = jnp.concatenate(
         [mine(w_receptance, 1), mine(w_key, 1), mine(w_value, 1), w_decay_down, w_rate_down], axis=1
     )
     w_conv = jnp.concatenate([mine(w_conv_gate, 1), mine(w_conv_in, 1), mine(w_conv_value, 1)], axis=1)
     w_out = jnp.concatenate([mine(w_out_conv, 0), mine(w_out_state, 0)], axis=0)
-    w_state = lax.all_gather(w_state, "sp", axis=0, tiled=True)
-    w_conv = lax.all_gather(w_conv, "sp", axis=0, tiled=True)
-    w_out = lax.all_gather(w_out, "sp", axis=0)
     shift = lax.all_to_all(
         decay_shift[0].reshape(steps, n_fs, width), "fs", split_axis=1, concat_axis=0
     ).reshape(n_fs, steps, width)
+    shift, local_tokens = lax.optimization_barrier((shift, normalize_rows(norm_gain, tokens[0])))
+    gathered = gather_inputs(n_sp, n_fs, n_tp, local_tokens, w_state)
+    normed, w_state, w_conv, w_out = lax.optimization_barrier((*gathered, w_conv, w_out))
+    normed = normed.reshape(n_fs * steps, normed.shape[-1])
+    w_state = w_state.reshape(-1, w_state.shape[-1])
+    w_conv = lax.all_gather(w_conv, "sp", axis=0, tiled=True)
+    w_out = lax.all_gather(w_out, "sp", axis=0)
 
     state_in = jnp.dot(normed, w_state, preferred_element_type=f32).astype(bf16)
     params = jnp.stack([mine(p, 0) for p in (decay_base, rate_base, key_scale, key_mix)])
@@ -249,10 +446,9 @@
     )(lax.axis_index("sp").reshape(1), query, local, ma_all, mine(group_gain, 0)[None])
 
     both = jnp.concatenate([conv_out, state_out], axis=1)
-    partial = jnp.concatenate(
-        [jnp.dot(both, w_out[j], preferred_element_type=f32).astype(bf16) for j in range(n_sp)], axis=1
-    )
-    mixed = lax.psum_scatter(partial, ("fs", "tp"), scatter_dimension=0, tiled=True)
+    w_out = jnp.swapaxes(w_out, 0, 1).reshape(both.shape[1], -1)
+    partial = jnp.dot(both, w_out, preferred_element_type=f32).astype(bf16)
+    mixed = reduce_partials(n_fs, partial.reshape(n_fs, n_tp, steps // n_tp, partial.shape[1]))
     return mixed[None]
 
 

time: 283 us -> 199 us (0.70)
  waiting for transfers between devices: 159 us -> 0.06 us
  Pallas kernels: 39.2 us -> 122 us
  local copies, waits for them, and re-layouts: 22.6 us -> 15.1 us
  blocking collectives: 14.4 us -> 21.2 us
  other arithmetic: 8.12 us -> 3.78 us
    all_gather x2 -> x0, waiting for transfers between devices: 87.1 us -> none  [the longest x1 47.1 us: body(): w_state = lax.all_gather(w_state, 'sp', axis=0, tiled=True)]
    pallas_call x0 -> x2, Pallas kernels: none -> 82.3 us  [the longest x1 48.4 us: gather_inputs(): pl.pallas_call(functools.partial(gather_kernel, n_sp, n_fs), in_specs=[pl...]
    unnamed x6 -> x2, waiting for transfers between devices: 54.8 us -> 0.03 us
    all_gather x1, waiting for transfers between devices: 16.8 us -> 0.02 us  [body(): w_conv = lax.all_gather(w_conv, 'sp', axis=0, tiled=True)]
    unnamed x21 -> x24, local copies, waits for them, and re-layouts: 13.5 us -> 6.14 us
    all_gather x1, blocking collectives: 14.4 us -> 21.2 us  [body(): ma_all = lax.all_gather(ma, 'sp', axis=0)]
    dot_general x4 -> x1, matrix products: 5.81 us -> 3.23 us  [body(): partial = jnp.dot(both, w_out, preferred_element_type=f32).astype(bf16)]
  transfers between devices with their start and end apart: 7 -> 4, of which waited for: 4 -> 0; matrix products, arithmetic and copies ran while one was open for 10% -> 14% of each run, Pallas kernels for 14% -> 20%
where the time goes in v1:
time: 199 us; the launch traced here: 196 us
  Pallas kernels  122 us (61%)
  blocking collectives  21.2 us (11%)
  matrix products  15.9 us (8%)
  local copies, waits for them, and re-layouts  15.1 us (8%)
  between operations  13.7 us (7%)
  starting transfers between devices  4.98 us (3%)
  other arithmetic  3.78 us (2%)
    pallas_call x1, Pallas kernels, gather_inputs(): pl.pallas_call(functools.partial(gather_kernel, n_sp, n_fs), in_specs=[pl...  48.4 us
    pallas_call x1, Pallas kernels, reduce_partials(): pl.pallas_call(functools.partial(reduce_kernel, n_fs), in_specs=[pl.Block...  33.9 us
    pallas_call x1, Pallas kernels, body(): pl.pallas_call(state_kernel, grid=(n_fs,), in_specs=[col(0), col(1), col(...  33.9 us
    all_gather x1, blocking collectives, body(): ma_all = lax.all_gather(ma, 'sp', axis=0)  21.2 us
    dot_general x1, matrix products, body(): state_in = jnp.dot(normed, w_state, preferred_element_type=f32).astype(bf16)  7.54 us
    unnamed x24, local copies, waits for them, and re-layouts  6.14 us
    pallas_call x1, Pallas kernels, body(): pl.pallas_call(functools.partial(finish_kernel, n_sp), grid=(n_fs,), in_s...  5.36 us
    dot_general x1, matrix products, body(): conv = jnp.dot(normed, w_conv, preferred_element_type=f32).astype(bf16)  5.1 us
  transfers between devices with their start and end apart: 4, of which 0 were waited for; matrix products, arithmetic and copies ran while one was open for 14% of the time, Pallas kernels for 20%

profile of v1, /device:TPU:25, one launch (start us, length us, event | category | flops | bytes accessed | tf_op | source)
XLA Modules:
  0.0 196.2 jit_solution(1694370526087520499)
XLA Ops:
  6.5 0.0 copy-start
  6.5 1.3 copy.27
  7.8 0.0 copy-start.6
  7.9 0.0 copy-start.7
  7.9 1.0 copy.28
  8.9 3.6 %all-to-all-start = ((f32[1,256,4,128]{3,1,0,2:T(8,128)}), f32[1,256,4,128]{3,1,0,2:T(8,128)S(1)}, u32[]{:S(2)}, u32[]{:S(2)}) async-start(f32[1,256,4,128]{3,1,0,2:T(8,128)} %copy.28), calls=%async_computation | async-start | bytes 1048576 | tf_op jit(solution)/shard_map/all_to_all | solution.py:385
  12.5 0.0 all-gather.5.cloned.1.call-start
  12.5 0.0 copy-done.1
  12.5 0.2 fusion
  12.7 0.9 dynamic-slice_dynamic-update-slice_fusion.2
  13.7 1.0 constant_dynamic-slice_fusion.6
  14.7 1.0 constant_dynamic-slice_fusion.3
  15.7 0.7 pad_maximum_fusion.1
  16.4 0.9 dynamic-slice_dynamic-update-slice_fusion.1
  17.4 1.0 dynamic-slice_dynamic-update-slice_fusion
  18.4 0.0 copy-done.6
  18.4 0.0 copy-done.7
  18.5 0.0 copy-start.3
  18.5 0.9 pad_maximum_fusion
  19.4 0.0 copy-done.8
  19.4 1.0 fusion.2.tok_ref
  20.4 0.0 all-to-all-done
  20.4 48.4 %shard_map.199 = (bf16[4,2,128,2048]{3,2,1,0:T(8,128)(2,1)}, bf16[4,512,640]{2,1,0:T(8,128)(2,1)}) custom-call(bf16[128,2048]{1,0:T(8,128)(2,1)} %fusion.2.tok_ref, bf16[512,640]{1,0:T(8,128)(2,1)} %copy-done.3), custom_call_target="tpu_custom_call" | custom-call | tf_op jit(solution)/shard_map/pallas_call | solution.py:334
  68.8 0.0 all-gather.5.cloned.1.call-update
  68.8 0.0 all-gather.7.cloned.1.call-start
  68.9 1.3 dynamic-slice_bitcast_fusion.gain_ref
  70.2 0.8 dynamic-slice_bitcast_fusion.3
  70.9 0.8 dynamic-slice_bitcast_fusion.1
  71.7 0.0 copy-done
  71.7 0.6 pad_maximum_fusion.3.par_ref
  72.3 1.4 constant_dynamic-slice_fusion
  73.7 7.5 %convolution_convert_fusion.1.recv_ref.key_ref.val_ref.dlow_ref.rlow_ref = bf16[1024,640]{1,0:T(8,128)(2,1)} fusion(bf16[1024,2048]{1,0:T(8,128)(2,1)} %bitcast.67, bf16[2048,640]{1,0:T(8,128)(2,1)} %bitcast.69), kind=kOutput, calls=%fused_computation.1 | convolution fusion | flops 2685009920 | bytes 8126464 | tf_op jit(solution)/shard_map/dot_general | solution.py:396
  81.3 0.0 all-gather.7.cloned.1.call-update
  81.3 33.9 %shard_map.200 = (bf16[1024,128]{1,0:T(8,128)(2,1)}, f32[1024,128]{1,0:T(8,128)}, bf16[4,2,64,128]{3,2,1,0:T(8,128)(2,1)}) custom-call(bf16[1024,640]{1,0:T(8,128)(2,1)} %convolution_convert_fusion.1.recv_ref.key_ref.val_ref.dlow_ref.rlow_ref, bf16[1024,640]{1,0:T(8,128)(2,1)} %convolution_convert_fusion.1.recv_ref.key_ref.val_ref.dlow_ref.rlow_ref, ...), custom_call_target="tpu_custom_call" | custom-call | flops 40000000000 | bytes 4000000 | tf_op jit(solution)/shard_map/pallas_call | solution.py:402
  115.2 0.0 all-gather.5.cloned.1.call-done
  115.2 5.1 %convolution_convert_fusion.2 = bf16[1024,384]{1,0:T(8,128)(2,1)S(1)} fusion(bf16[1024,2048]{1,0:T(8,128)(2,1)} %bitcast.68, bf16[2048,384]{1,0:T(8,128)(2,1)} %all-gather.5.cloned.1.call-done), kind=kOutput, calls=%fused_computation.2 | convolution fusion | flops 1611005952 | bytes 6553600 | tf_op jit(solution)/shard_map/dot_general | solution.py:424
  120.3 0.1 fusion.11
  120.5 1.3 collective-permute-start
  121.8 21.2 %all-gather = bf16[16,2,64,128]{3,2,1,0:T(8,128)(2,1)} all-gather(bf16[4,2,64,128]{3,2,1,0:T(8,128)(2,1)S(1)} %copy-done.5), channel_id=2, replica_groups=mesh['sp'=4,'fs'=4,'tp'=2] {'sp'}, dimensions={0}, use_global_device_ids=true | all-gather | bytes 655360 | tf_op jit(solution)/shard_map/all_gather | solution.py:422
  143.0 5.4 %shard_map.201 = bf16[1024,128]{1,0:T(8,128)(2,1)} custom-call(s32[1]{0:T(128)} %bitcast.18.place_ref, bf16[1024,128]{1,0:T(8,128)(2,1)} %get-tuple-element.23.q_ref, f32[1024,128]{1,0:T(8,128)} %get-tuple-element.24.l_ref, bf16[4,4,2,64,128]{4,3,2,1,0:T(8,128)(2,1)} %bitcast.57, f32[1,128]{1,0:T(1,128)} %dynamic-slice_bitcast_fusion.gain_ref), custom_call_target="tpu_custom_call" | custom-call | tf_op jit(solution)/shard_map/pallas_call | solution.py:437
  148.4 1.5 copy.29
  149.9 0.0 collective-permute-done
  150.0 0.1 convert_multiply_fusion.2
  150.1 0.2 fusion.5
  150.3 0.0 copy-done.2
  150.3 3.2 %convolution_convert_fusion = bf16[1024,2048]{1,0:T(8,128)(2,1)} fusion(bf16[256,2048]{0,1:T(8,128)(2,1)S(1)} %bitcast.55, bf16[1024,128]{1,0:T(8,128)(2,1)S(1)} %copy-done.2, bf16[1024,128]{1,0:T(8,128)(2,1)S(1)} %bitcast.63), kind=kOutput, calls=%fused_computation | convolution fusion | flops 1076887552 | bytes 5767168 | tf_op jit(solution)/shard_map/dot_general | solution.py:450
  153.6 33.9 %shard_map.202 = bf16[128,2048]{1,0:T(8,128)(2,1)} custom-call(bf16[4,2,128,2048]{3,2,1,0:T(8,128)(2,1)} %bitcast.54), custom_call_target="tpu_custom_call" | custom-call | tf_op jit(solution)/shard_map/pallas_call | solution.py:350
  187.5 1.9 copy.35
  (18 shorter events, 0.1 us)
Async XLA Ops:
  6.5 65.2 %copy-start = (f32[3,512]{1,0:T(4,128)S(1)}, f32[3,512]{1,0:T(4,128)}, u32[]{:S(2)}) copy-start(f32[3,512]{1,0:T(4,128)} %param.26) | copy-start | bytes 18436
  6.5 6.0 %copy-start.1 = (bf16[1,128,2048]{2,1,0:T(8,128)(2,1)S(1)}, bf16[1,128,2048]{2,1,0:T(8,128)(2,1)}, u32[]{:S(2)}) copy-start(bf16[1,128,2048]{2,1,0:T(8,128)(2,1)} %param.21) | copy-start | bytes 1572868
  7.8 10.5 %copy-start.6 = (bf16[512,128]{1,0:T(8,128)(2,1)S(1)}, bf16[512,128]{1,0:T(8,128)(2,1)}, u32[]{:S(2)}) copy-start(bf16[512,128]{1,0:T(8,128)(2,1)} %param.30) | copy-start | bytes 393220
  7.9 10.6 %copy-start.7 = (bf16[512,128]{1,0:T(8,128)(2,1)S(1)}, bf16[512,128]{1,0:T(8,128)(2,1)}, u32[]{:S(2)}) copy-start(bf16[512,128]{1,0:T(8,128)(2,1)} %param.34) | copy-start | bytes 393220
  8.9 10.5 %copy-start.8 = (f32[2048]{0:T(1024)S(1)}, f32[2048]{0:T(1024)}, u32[]{:S(2)}) copy-start(f32[2048]{0:T(1024)} %param.22) | copy-start | bytes 24580
  8.9 11.5 %all-to-all-start = ((f32[1,256,4,128]{3,1,0,2:T(8,128)}), f32[1,256,4,128]{3,1,0,2:T(8,128)S(1)}, u32[]{:S(2)}, u32[]{:S(2)}) async-start(f32[1,256,4,128]{3,1,0,2:T(8,128)} %copy.28), calls=%async_computation | async-start | bytes 1048576 | tf_op jit(solution)/shard_map/all_to_all | solution.py:385
  12.5 102.7 %all-gather.5.cloned.1.call-start = ((), (), s32[]{:S(2)}) async-start(), calls=%async_computation.1 | async-start | bytes 1966080 | tf_op jit(solution)/shard_map/all_gather | solution.py:393
  18.5 1.9 copy-start.3
  20.4 60.9 %copy-start.4 = (f32[1,256,4,128]{3,1,0,2:T(8,128)}, f32[1,256,4,128]{3,1,0,2:T(8,128)S(1)}, u32[]{:S(2)}) copy-start(f32[1,256,4,128]{3,1,0,2:T(8,128)S(1)} %all-to-all-done) | copy-start | bytes 1572868
  68.8 79.6 %all-gather.7.cloned.1.call-start = ((), (), s32[]{:S(2)}) async-start(), calls=%async_computation.2 | async-start | bytes 1310720 | tf_op jit(solution)/shard_map/all_gather | solution.py:394
  115.2 6.6 %copy-start.5 = (bf16[4,2,64,128]{3,2,1,0:T(8,128)(2,1)S(1)}, bf16[4,2,64,128]{3,2,1,0:T(8,128)(2,1)}, u32[]{:S(2)}) copy-start(bf16[4,2,64,128]{3,2,1,0:T(8,128)(2,1)} %get-tuple-element.25) | copy-start | bytes 393220
  120.5 29.4 %collective-permute-start = (bf16[2,4,2,128]{3,2,1,0:T(2,128)(2,1)S(1)}, bf16[2,4,2,128]{3,2,1,0:T(2,128)(2,1)S(1)}, u32[]{:S(2)}, u32[]{:S(2)}) collective-permute-start(bf16[2,4,2,128]{3,2,1,0:T(2,128)(2,1)S(1)} %pad_maximum_fusion.2), channel_id=1, source_target_pairs={{0,8},{8,16},{16,24},{1,9},{9,17},{17,25},{2,10},{10,18},{18,26},{... | collective-permute-start | bytes 12296 | tf_op jit(solution)/shard_map/ppermute | solution.py:429
  148.4 1.9 copy-start.2
Sparse Core Ops, SparseCore 0:
  68.9 37.7 all-gather.4
  108.3 36.3 all-gather.6

commit v2 on v1

--- a/solution.py
+++ b/solution.py
@@ -100,21 +100,29 @@
         tail = jnp.exp(final - incl)
         r_end = st(replace[sl] * tail)
         k_end = st(write[sl] * tail)
-        x = jnp.where(strict, dot3(e_mid, r_back, NT), 0.0)
-        ek = jnp.where(strict, dot1(e_mid, k_back, NT), 0.0)
-        qr = jnp.where(causal, dot1(q_mid, r_back, NT), 0.0)
-        qk = jnp.where(causal, dot1(q_mid, k_back, NT), 0.0)
+        pairs = dot1(
+            jnp.concatenate([e_mid, q_mid], axis=0), jnp.concatenate([r_back, k_back], axis=0), NT
+        )
+        x = jnp.where(strict, pairs[:rows, :rows], 0.0)
+        ek = jnp.where(strict, pairs[:rows, rows:], 0.0)
+        qr = jnp.where(causal, pairs[rows:, :rows], 0.0)
+        qk = jnp.where(causal, pairs[rows:, rows:], 0.0)
+        ekv_qkv = dot1(jnp.concatenate([ek, qk], axis=0), v, NN)
         inv = eye + x
-        power = x
+        power = dot1(x, x, NN)
         reached = 2
         while reached < CHUNK:
-            power = dot3(power, power, NN)
-            inv = inv + dot3(inv, power, NN)
+            if reached * 2 < CHUNK:
+                step = dot1(jnp.concatenate([inv, power], axis=0), power, NN)
+                inv, power = inv + step[:rows], step[rows:]
+            else:
+                inv = inv + dot1(inv, power, NN)
             reached *= 2
-        start_map = dot3(inv, e_now, NN)
-        local_erase = dot1(inv, dot1(ek, v, NN), NN)
-        query_map = fold(q_now + dot1(qr, start_map, NN))
-        local_out = fold(dot1(qr, local_erase, NN) + dot1(qk, v, NN))
+        solved = dot1(inv, jnp.concatenate([e_now, ekv_qkv[:rows]], axis=1), NN)
+        start_map, local_erase = solved[:, :width], solved[:, width:]
+        seen = dot1(qr, solved, NN)
+        query_map = fold(q_now + seen[:, :width])
+        local_out = fold(seen[:, width:] + ekv_qkv[rows:])
         decay_diag = jnp.where(weye, jnp.exp(final), 0.0)
         step_map = decay_diag + dot3(start_map, r_end, TN)
         carried = dot1(local_erase, r_end, TN) + dot1(v, k_end, TN)
@@ -182,12 +190,33 @@
 
 
 def gather_kernel(
-    n_sp, n_fs, tok_ref, w_ref, toks, weights, local_sem, tok_send, tok_recv, pair_send, pair_recv,
-    right_send, left_send, w_recv,
+    n_sp, n_fs, tok_ref, shift_ref, *refs
 ):
+    w_refs, refs = refs[:5], refs[5:]
+    (
+        toks, weights, shifts, w_sem, local_sem, tok_send, tok_recv, pair_send, pair_recv,
+        right_send, left_send, w_recv, shift_send, shift_recv,
+    ) = refs
+    width = shifts.shape[-1]
     sp, fs, tp = lax.axis_index("sp"), lax.axis_index("fs"), lax.axis_index("tp")
     partner = {"tp": 1 - tp}
     others = [lax.rem(fs + d, n_fs) for d in range(1, n_fs)]
+    start_lane, pieces = 0, []
+    for k, ref in enumerate(w_refs):
+        wide = width if k < 3 else ref.shape[1]
+        source = ref.at[:, pl.ds(pl.multiple_of(fs * width, width), width)] if k < 3 else ref
+        pieces.append(
+            pltpu.make_async_copy(
+                source, weights.at[sp, :, pl.ds(start_lane, wide)], w_sem.at[k]
+            )
+        )
+        start_lane += wide
+    for piece in pieces:
+        piece.start()
+
+    def shift_block(f):
+        return shift_ref.at[:, pl.ds(pl.multiple_of(f * width, width), width)]
+
     barrier = greet([partner] + [{"fs": f} for f in others])
     has_left, has_right = sp > 0, sp < n_sp - 1
 
@@ -209,8 +238,9 @@
         src = weights.at[j]
         return send(src, weights.at[j], left_send.at[j], w_recv.at[j], {"sp": sp - 1})
 
-    own_right = send(w_ref, weights.at[sp], right_send.at[sp], w_recv.at[sp], {"sp": sp + 1})
-    own_left = send(w_ref, weights.at[sp], left_send.at[sp], w_recv.at[sp], {"sp": sp - 1})
+    own_right, own_left = rightward(sp), leftward(sp)
+    for piece in pieces:
+        piece.wait()
 
     @pl.when(has_right)
     def _():
@@ -220,9 +250,9 @@
     def _():
         own_left.start()
 
-    own_w = pltpu.make_async_copy(w_ref, weights.at[sp], local_sem.at[0])
+    own_s = pltpu.make_async_copy(shift_block(fs), shifts.at[fs], local_sem.at[0])
     own_t = pltpu.make_async_copy(tok_ref, toks.at[fs, tp], local_sem.at[1])
-    own_w.start()
+    own_s.start()
     own_t.start()
     token_sends = [
         send(tok_ref, toks.at[fs, tp], tok_send.at[f], tok_recv.at[fs], {"fs": f}) for f in others
@@ -231,6 +261,12 @@
         copy.start()
     pair_own = send(tok_ref, toks.at[fs, tp], pair_send.at[fs], pair_recv.at[fs], partner)
     pair_own.start()
+    shift_sends = [
+        send(shift_block(f), shifts.at[fs], shift_send.at[f], shift_recv.at[fs], {"fs": f})
+        for f in others
+    ]
+    for copy in shift_sends:
+        copy.start()
 
     def from_peer(f):
         return send(toks.at[f, tp], toks.at[f, tp], tok_send.at[f], tok_recv.at[f], {"fs": f})
@@ -265,10 +301,12 @@
                 from_peer(f).wait_recv()
                 to_partner(f).start()
 
-    own_w.wait()
+    own_s.wait()
     own_t.wait()
-    for copy in token_sends:
+    for copy in token_sends + shift_sends:
         copy.wait_send()
+    for f in others:
+        send(shifts.at[f], shifts.at[f], shift_send.at[f], shift_recv.at[f], {"fs": f}).wait_recv()
     pair_own.wait_send()
     for f in others:
         to_partner(f).wait_send()
@@ -329,19 +367,68 @@
         copy.wait_send()
 
 
-def gather_inputs(n_sp, n_fs, n_tp, tok, w):
+def gather_inputs(n_sp, n_fs, n_tp, tok, shift, weights):
     dma = lambda n: pltpu.SemaphoreType.DMA((n,))
+    depth, width = weights[0].shape[0], weights[0].shape[1] // n_fs
+    columns = 3 * width + weights[3].shape[1] + weights[4].shape[1]
+    vmem = pl.BlockSpec(memory_space=pltpu.VMEM)
     return pl.pallas_call(
         functools.partial(gather_kernel, n_sp, n_fs),
-        in_specs=[pl.BlockSpec(memory_space=pltpu.VMEM)] * 2,
-        out_specs=[pl.BlockSpec(memory_space=pltpu.VMEM)] * 2,
+        in_specs=[vmem, vmem] + [pl.BlockSpec(memory_space=pl.ANY)] * 5,
+        out_specs=[vmem] * 3,
         out_shape=[
             jax.ShapeDtypeStruct((n_fs, n_tp) + tok.shape, bf16),
-            jax.ShapeDtypeStruct((n_sp,) + w.shape, bf16),
+            jax.ShapeDtypeStruct((n_sp, depth, columns), bf16),
+            jax.ShapeDtypeStruct((n_fs, shift.shape[0], width), f32),
         ],
-        scratch_shapes=[dma(2), dma(n_fs), dma(n_fs), dma(n_fs), dma(n_fs), dma(n_sp), dma(n_sp), dma(n_sp)],
+        scratch_shapes=[dma(5), dma(2)] + [dma(n_fs)] * 4 + [dma(n_sp)] * 3 + [dma(n_fs)] * 2,
         compiler_params=pltpu.CompilerParams(collective_id=0, has_side_effects=True),
-    )(tok, w)
+    )(tok, shift, *weights)
+
+
+def map_kernel(n_sp, ma_ref, out_ref, send_sem, recv_sem):
+    sp = lax.axis_index("sp")
+    barrier = pltpu.get_barrier_semaphore()
+    for k in range(1, n_sp):
+
+        @pl.when(sp >= k)
+        def _():
+            pl.semaphore_signal(barrier, inc=1, device_id={"sp": sp - k}, device_id_type=MESH)
+
+    @pl.when(sp < n_sp - 1)
+    def _():
+        pl.semaphore_wait(barrier, n_sp - 1 - sp)
+
+    def later(k):
+        return send(ma_ref, out_ref.at[sp], send_sem.at[k], recv_sem.at[sp], {"sp": sp + k})
+
+    for k in range(1, n_sp):
+
+        @pl.when(sp + k < n_sp)
+        def _():
+            later(k).start()
+
+    for k in range(1, n_sp):
+
+        @pl.when(sp >= k)
+        def _():
+            slot = out_ref.at[sp - k]
+            send(slot, slot, send_sem.at[0], recv_sem.at[sp - k], {"sp": sp - k}).wait_recv()
+
+        @pl.when(sp + k < n_sp)
+        def _():
+            later(k).wait_send()
+
+
+def earlier_maps(n_sp, ma):
+    return pl.pallas_call(
+        functools.partial(map_kernel, n_sp),
+        in_specs=[pl.BlockSpec(memory_space=pltpu.VMEM)],
+        out_specs=pl.BlockSpec(memory_space=pltpu.VMEM),
+        out_shape=jax.ShapeDtypeStruct((n_sp,) + ma.shape, bf16),
+        scratch_shapes=[pltpu.SemaphoreType.DMA((n_sp,))] * 2,
+        compiler_params=pltpu.CompilerParams(collective_id=2, has_side_effects=True),
+    )(ma)
 
 
 def reduce_partials(n_fs, part):
@@ -377,17 +464,13 @@
 
     n_tp = lax.axis_size("tp")
     steps = decay_shift.shape[1]
-    w_state = jnp.concatenate(
-        [mine(w_receptance, 1), mine(w_key, 1), mine(w_value, 1), w_decay_down, w_rate_down], axis=1
-    )
     w_conv = jnp.concatenate([mine(w_conv_gate, 1), mine(w_conv_in, 1), mine(w_conv_value, 1)], axis=1)
     w_out = jnp.concatenate([mine(w_out_conv, 0), mine(w_out_state, 0)], axis=0)
-    shift = lax.all_to_all(
-        decay_shift[0].reshape(steps, n_fs, width), "fs", split_axis=1, concat_axis=0
-    ).reshape(n_fs, steps, width)
-    shift, local_tokens = lax.optimization_barrier((shift, normalize_rows(norm_gain, tokens[0])))
-    gathered = gather_inputs(n_sp, n_fs, n_tp, local_tokens, w_state)
-    normed, w_state, w_conv, w_out = lax.optimization_barrier((*gathered, w_conv, w_out))
+    normed, w_state, shift = gather_inputs(
+        n_sp, n_fs, n_tp, normalize_rows(norm_gain, tokens[0]), decay_shift[0],
+        (w_receptance, w_key, w_value, w_decay_down, w_rate_down),
+    )
+    normed, w_state, w_conv, w_out = lax.optimization_barrier((normed, w_state, w_conv, w_out))
     normed = normed.reshape(n_fs * steps, normed.shape[-1])
     w_state = w_state.reshape(-1, w_state.shape[-1])
     w_conv = lax.all_gather(w_conv, "sp", axis=0, tiled=True)
@@ -419,7 +502,7 @@
         state_in, state_in, state_in, state_in, state_in, mine(w_decay_up, 1), mine(w_rate_up, 1),
         shift, params,
     )
-    ma_all = lax.all_gather(ma, "sp", axis=0)
+    ma_all = earlier_maps(n_sp, ma)
 
     conv = jnp.dot(normed, w_conv, preferred_element_type=f32).astype(bf16)
     gate, source, value = (

time: 199 us -> 192 us (0.965)
  Pallas kernels: 122 us -> 144 us
  blocking collectives: 21.2 us -> 0 us
  local copies, waits for them, and re-layouts: 15.1 us -> 10.5 us
  starting transfers between devices: 4.98 us -> 1.34 us
    pallas_call x1 -> x2, Pallas kernels: 48.4 us -> 77 us  [the longest x1 48.6 us: gather_inputs(): pl.pallas_call(functools.partial(gather_kernel, n_sp, n_fs), in_specs=[vm...]
    all_gather x1 -> x0, blocking collectives: 21.2 us -> none  [body(): ma_all = lax.all_gather(ma, 'sp', axis=0)]
    pallas_call x1, Pallas kernels: 33.9 us -> 29 us  [body(): pl.pallas_call(state_kernel, grid=(n_fs,), in_specs=[col(0), col(1), col(...]
    unnamed x24 -> x7, local copies, waits for them, and re-layouts: 6.14 us -> 1.89 us
    all_to_all x1 -> x0, starting transfers between devices: 3.6 us -> none  [body(): lax.all_to_all(decay_shift[0].reshape(steps, n_fs, width), 'fs', split_ax...]
    dynamic_slice x4 -> x5, local copies, waits for them, and re-layouts: 3.4 us -> 4.11 us  [mine(): return lax.dynamic_slice_in_dim(a, fs * width, width, axis)]
  transfers between devices with their start and end apart: 4 -> 3, of which waited for: 0 -> 0; matrix products, arithmetic and copies ran while one was open for 14% -> 10% of each run, Pallas kernels for 20% -> 33%
where the time goes in v2:
time: 192 us; the launch traced here: 191 us
  Pallas kernels  144 us (75%)
  matrix products  15.8 us (8%)
  between operations  13.6 us (7%)
  local copies, waits for them, and re-layouts  10.5 us (5%)
  other arithmetic  5.46 us (3%)
    pallas_call x1, Pallas kernels, gather_inputs(): pl.pallas_call(functools.partial(gather_kernel, n_sp, n_fs), in_specs=[vm...  48.6 us
    pallas_call x1, Pallas kernels, reduce_partials(): pl.pallas_call(functools.partial(reduce_kernel, n_fs), in_specs=[pl.Block...  32.2 us
    pallas_call x1, Pallas kernels, body(): pl.pallas_call(state_kernel, grid=(n_fs,), in_specs=[col(0), col(1), col(...  29 us
    pallas_call x1, Pallas kernels, earlier_maps(): pl.pallas_call(functools.partial(map_kernel, n_sp), in_specs=[pl.BlockSpe...  28.4 us
    dot_general x1, matrix products, body(): state_in = jnp.dot(normed, w_state, preferred_element_type=f32).astype(bf16)  7.57 us
    pallas_call x1, Pallas kernels, body(): pl.pallas_call(functools.partial(finish_kernel, n_sp), grid=(n_fs,), in_s...  5.38 us
    dot_general x1, matrix products, body(): conv = jnp.dot(normed, w_conv, preferred_element_type=f32).astype(bf16)  5 us
    dynamic_slice x5, local copies, waits for them, and re-layouts, mine(): return lax.dynamic_slice_in_dim(a, fs * width, width, axis)  4.11 us
  transfers between devices with their start and end apart: 3, of which 0 were waited for; matrix products, arithmetic and copies ran while one was open for 10% of the time, Pallas kernels for 33%

profile of v2, /device:TPU:25, one launch (start us, length us, event | category | flops | bytes accessed | tf_op | source)
XLA Modules:
  0.0 191.0 jit_solution(6073814934034247704)
XLA Ops:
  6.5 0.0 copy-start
  6.5 0.0 copy-start.1
  6.5 0.0 all-gather.4.cloned.1.call-start
  6.5 1.3 fusion
  7.9 0.0 copy-done
  7.9 1.0 constant_dynamic-slice_fusion.5
  8.9 1.0 constant_dynamic-slice_fusion.3
  9.9 0.7 pad_maximum_fusion.1
  10.6 0.0 copy-done.1
  10.6 1.7 fusion.2.tok_ref
  12.3 0.8 pad_maximum_fusion
  13.1 48.6 %shard_map.199 = (bf16[4,2,128,2048]{3,2,1,0:T(8,128)(2,1)}, bf16[4,512,640]{2,1,0:T(8,128)(2,1)}, f32[4,256,128]{2,1,0:T(8,128)}) custom-call(bf16[128,2048]{1,0:T(8,128)(2,1)} %fusion.2.tok_ref, f32[256,512]{1,0:T(8,128)} %bitcast.58, bf16[512,512]{1,0:T(8,128)(2,1)} %refs_0_.1, bf16[512,512]{1,0:T(8,128)(2,1)} %refs_1_.1, bf16[512,512]{1,0:T(8,128)(2,1)} %refs_2_.1, ...), custom_call_target="tpu_custom_call" | custom-call | tf_op jit(solution)/shard_map/pallas_call | solution.py:375
  61.7 0.0 all-gather.4.cloned.1.call-update
  61.7 0.0 all-gather.6.cloned.1.call-start
  61.7 0.7 all-gather.6.cloned.1.call-update
  62.4 0.7 constant_dynamic-slice_fusion.2
  63.1 0.8 dynamic-slice_bitcast_fusion.3
  63.9 0.8 dynamic-slice_bitcast_fusion.1
  64.7 1.4 constant_dynamic-slice_fusion
  66.1 7.6 %convolution_convert_fusion.1.recv_ref.key_ref.val_ref.dlow_ref.rlow_ref = bf16[1024,640]{1,0:T(8,128)(2,1)} fusion(bf16[1024,2048]{1,0:T(8,128)(2,1)} %bitcast.59, bf16[2048,640]{1,0:T(8,128)(2,1)} %bitcast.61), kind=kOutput, calls=%fused_computation.1 | convolution fusion | flops 2685009920 | bytes 8126464 | tf_op jit(solution)/shard_map/dot_general | solution.py:479
  73.6 0.6 pad_maximum_fusion.3.par_ref
  74.2 29.0 %shard_map.200 = (bf16[1024,128]{1,0:T(8,128)(2,1)}, f32[1024,128]{1,0:T(8,128)}, bf16[4,2,64,128]{3,2,1,0:T(8,128)(2,1)}) custom-call(bf16[1024,640]{1,0:T(8,128)(2,1)} %convolution_convert_fusion.1.recv_ref.key_ref.val_ref.dlow_ref.rlow_ref, bf16[1024,640]{1,0:T(8,128)(2,1)} %convolution_convert_fusion.1.recv_ref.key_ref.val_ref.dlow_ref.rlow_ref, ...), custom_call_target="tpu_custom_call" | custom-call | flops 40000000000 | bytes 4000000 | tf_op jit(solution)/shard_map/pallas_call | solution.py:485
  103.3 0.0 all-gather.4.cloned.1.call-done
  103.3 5.0 %convolution_convert_fusion.2 = bf16[1024,384]{1,0:T(8,128)(2,1)S(1)} fusion(bf16[1024,2048]{1,0:T(8,128)(2,1)} %bitcast.60, bf16[2048,384]{1,0:T(8,128)(2,1)} %all-gather.4.cloned.1.call-done), kind=kOutput, calls=%fused_computation.2 | convolution fusion | flops 1611005952 | bytes 6553600 | tf_op jit(solution)/shard_map/dot_general | solution.py:507
  108.3 0.1 fusion.11
  108.5 1.3 collective-permute-start
  109.8 1.3 dynamic-slice_bitcast_fusion.gain_ref
  111.1 28.4 %shard_map.201.ma_ref = bf16[4,4,2,64,128]{4,3,2,1,0:T(8,128)(2,1)} custom-call(bf16[4,2,64,128]{3,2,1,0:T(8,128)(2,1)} %get-tuple-element.23.ma_ref), custom_call_target="tpu_custom_call" | custom-call | tf_op jit(solution)/shard_map/pallas_call | solution.py:424
  139.5 5.4 %shard_map.202 = bf16[1024,128]{1,0:T(8,128)(2,1)} custom-call(s32[1]{0:T(128)} %bitcast.15.place_ref, bf16[1024,128]{1,0:T(8,128)(2,1)} %get-tuple-element.21.q_ref, f32[1024,128]{1,0:T(8,128)} %get-tuple-element.22.l_ref, bf16[4,4,2,64,128]{4,3,2,1,0:T(8,128)(2,1)} %shard_map.201.ma_ref, f32[1,128]{1,0:T(1,128)} %dynamic-slice_bitcast_fusion.gain_ref), custom_call_target="tpu_custom_call" | custom-call | tf_op jit(solution)/shard_map/pallas_call | solution.py:520
  144.9 0.0 all-gather.6.cloned.1.call-done
  144.9 0.0 copy-start.2
  144.9 1.5 copy.22
  146.4 0.0 collective-permute-done
  146.4 0.1 convert_multiply_fusion.2
  146.6 0.2 fusion.5
  146.8 0.0 copy-done.2
  146.8 3.3 %convolution_convert_fusion = bf16[1024,2048]{1,0:T(8,128)(2,1)} fusion(bf16[256,2048]{0,1:T(8,128)(2,1)S(1)} %bitcast.49, bf16[1024,128]{1,0:T(8,128)(2,1)S(1)} %copy-done.2, bf16[1024,128]{1,0:T(8,128)(2,1)S(1)} %bitcast.55), kind=kOutput, calls=%fused_computation | convolution fusion | flops 1076887552 | bytes 5767168 | tf_op jit(solution)/shard_map/dot_general | solution.py:533
  150.0 32.2 %shard_map.203 = bf16[128,2048]{1,0:T(8,128)(2,1)} custom-call(bf16[4,2,128,2048]{3,2,1,0:T(8,128)(2,1)} %bitcast.48), custom_call_target="tpu_custom_call" | custom-call | tf_op jit(solution)/shard_map/pallas_call | solution.py:437
  182.2 1.9 copy.24
  (7 shorter events, 0.1 us)
Async XLA Ops:
  6.5 1.3 copy-start
  6.5 4.1 %copy-start.1 = (bf16[1,128,2048]{2,1,0:T(8,128)(2,1)S(1)}, bf16[1,128,2048]{2,1,0:T(8,128)(2,1)}, u32[]{:S(2)}) copy-start(bf16[1,128,2048]{2,1,0:T(8,128)(2,1)} %param.21) | copy-start | bytes 1572868
  6.5 96.8 %all-gather.4.cloned.1.call-start = ((), (), s32[]{:S(2)}) async-start(), calls=%async_computation | async-start | bytes 1966080 | tf_op jit(solution)/shard_map/all_gather | solution.py:476
  61.7 83.2 %all-gather.6.cloned.1.call-start = ((), (), s32[]{:S(2)}) async-start(), calls=%async_computation.1 | async-start | bytes 1310720 | tf_op jit(solution)/shard_map/all_gather | solution.py:477
  108.5 37.9 %collective-permute-start = (bf16[2,4,2,128]{3,2,1,0:T(2,128)(2,1)S(1)}, bf16[2,4,2,128]{3,2,1,0:T(2,128)(2,1)S(1)}, u32[]{:S(2)}, u32[]{:S(2)}) collective-permute-start(bf16[2,4,2,128]{3,2,1,0:T(2,128)(2,1)S(1)} %pad_maximum_fusion.2), channel_id=1, source_target_pairs={{0,8},{8,16},{16,24},{1,9},{9,17},{17,25},{2,10},{10,18},{18,26},{... | collective-permute-start | bytes 12296 | tf_op jit(solution)/shard_map/ppermute | solution.py:512
  144.9 1.9 copy-start.2
Sparse Core Ops, SparseCore 0:
  61.8 37.2 all-gather.3
  100.6 38.0 all-gather.5
